TPU v7x, 32 devices: a whole 2x2x4 slice. The times are simulated.
32 devices in a mesh: sp: 8 (over z, y), tp: 4 (over x, core).
Axes of the slice: x: 2, y: 2, z: 4, core: 2. Of those that a mesh axis runs over, the one named last changes fastest.
Arguments:
- queries: bfloat16 [2048, 2048], P('sp', 'tp'), may hold values from -6 to 6
- key_value: bfloat16 [2048, 4, 128], P('sp', 'tp'), may hold values from -12 to 12
- break_bias: bfloat16 [2048, 32], P('sp', 'tp'), may hold values from -13 to 0
- stream: bfloat16 [2048, 2048], P(('sp', 'tp')), may hold values from -6 to 6
- out_proj: bfloat16 [2048, 2048], replicated, may hold values from -0.125 to 0.125
- ffn_gain: float32 [2048], replicated, may hold values from 0.1 to 1.9
- routes: int32 [2048, 4], P(('sp', 'tp')), may hold values from 0 to 31, all different within a row; in each aligned block of 64 rows (0 to 63, 64 to 127, ...) at most 16 rows name the same one
- route_score: float32 [2048, 4], P(('sp', 'tp')), may hold values from 0.05 to 1
- expert_gate: bfloat16 [32, 2048, 512], P(('sp', 'tp')), may hold values from -0.125 to 0.125
- expert_up: bfloat16 [32, 2048, 512], P(('sp', 'tp')), may hold values from -0.125 to 0.125
- expert_down: bfloat16 [32, 512, 2048], P(('sp', 'tp')), may hold values from -0.25 to 0.25
- shared_gate: bfloat16 [2048, 512], replicated, may hold values from -0.125 to 0.125
- shared_up: bfloat16 [2048, 512], replicated, may hold values from -0.125 to 0.125
- shared_down: bfloat16 [512, 2048], replicated, may hold values from -0.25 to 0.25
Outputs:
- layer_out: bfloat16 [2048, 2048], P(('sp', 'tp'))
Inputs may be any that keep to these rules, and one draw needn't show every extreme that they name: `routes`: each row names 4 different experts. In each aligned block of 64 rows (the rows of one device) no expert is named by more than 16 rows, a bound that some block reaches.
All inputs are finite; a program needn't handle non-finite values.
Results may differ from a plain program's by a relative error of at most 0.015.
Values may be sent and summed in bfloat16 or wider, within the bound.
A program may use at most 128 MiB of HBM per device.

v0:
```python
import functools
import math

import jax
import jax.numpy as jnp
from jax import lax
from jax.experimental import pallas as pl
from jax.experimental.pallas import tpu as pltpu
from jax.sharding import PartitionSpec as P

MESH = pl.DeviceIdType.MESH
LOG2E = math.log2(math.e)
HEADS_AT_ONCE = 4


def gather_kernel(seq, half, packed_ref, query_ref, route_ref, every_ref, far_ref, plans_ref,
                  send, recv, q_send, q_recv, r_send, r_recv):
    me = lax.axis_index("sp")
    partner = me + 1 - 2 * (me % 2)
    mirror = seq - 1 - me
    barrier = pltpu.get_barrier_semaphore()
    for step in range(1, seq):
        pl.semaphore_signal(
            barrier, inc=1, device_id={"sp": (me + step) % seq}, device_id_type=MESH
        )
    pl.semaphore_wait(barrier, seq - 1)

    def push(source, block, target, slot):
        return pltpu.make_async_remote_copy(
            src_ref=source,
            dst_ref=every_ref.at[block],
            send_sem=send.at[slot],
            recv_sem=recv.at[block],
            device_id={"sp": target},
            device_id_type=MESH,
        )

    steps = seq // 2
    first = [push(packed_ref, me, partner, 0)]
    for step in range(1, steps):
        first.append(push(packed_ref, me, (me + 2 * step) % seq, step))
    for copy in first:
        copy.start()
    send_start = jnp.where(me < seq // 2, half, 0)
    moving = pltpu.make_async_remote_copy(
        src_ref=query_ref.at[pl.ds(pl.multiple_of(send_start, half), half)],
        dst_ref=far_ref,
        send_sem=q_send,
        recv_sem=q_recv,
        device_id={"sp": mirror},
        device_id_type=MESH,
    )
    moving.start()

    def tell(step):
        return pltpu.make_async_remote_copy(
            src_ref=route_ref,
            dst_ref=plans_ref.at[me],
            send_sem=r_send.at[step],
            recv_sem=r_recv.at[me],
            device_id={"sp": (me + step) % seq},
            device_id_type=MESH,
        )

    for step in range(1, seq):
        tell(step).start()
    plans_ref[me] = route_ref[...]
    every_ref[me] = packed_ref[...]
    relayed = []
    for step in range(1, steps):
        block = (me + seq - 2 * step) % seq
        copy = push(every_ref.at[block], block, partner, steps + step)
        push(packed_ref, block, partner, 0).wait_recv()
        copy.start()
        relayed.append(copy)
    for step in range(steps):
        block = (partner + seq - 2 * step) % seq
        push(packed_ref, block, partner, 0).wait_recv()
    moving.wait_recv()
    for step in range(1, seq):
        block = (me + step) % seq
        pltpu.make_async_remote_copy(
            src_ref=route_ref,
            dst_ref=plans_ref.at[block],
            send_sem=r_send.at[step],
            recv_sem=r_recv.at[block],
            device_id={"sp": block},
            device_id_type=MESH,
        ).wait_recv()
    for copy in first + relayed:
        copy.wait_send()
    for step in range(1, seq):
        tell(step).wait_send()
    moving.wait_send()


def gather_keys(packed, queries, route, seq):
    half = queries.shape[0] // 2
    vmem = pl.BlockSpec(memory_space=pltpu.VMEM)
    return pl.pallas_call(
        functools.partial(gather_kernel, seq, half),
        out_shape=(
            jax.ShapeDtypeStruct((seq,) + packed.shape, packed.dtype),
            jax.ShapeDtypeStruct((half, queries.shape[1]), queries.dtype),
            jax.ShapeDtypeStruct((seq,) + route.shape, route.dtype),
        ),
        in_specs=[vmem, vmem, vmem],
        out_specs=(vmem, vmem, vmem),
        scratch_shapes=[
            pltpu.SemaphoreType.DMA((seq,)),
            pltpu.SemaphoreType.DMA((seq,)),
            pltpu.SemaphoreType.DMA,
            pltpu.SemaphoreType.DMA,
            pltpu.SemaphoreType.DMA((seq,)),
            pltpu.SemaphoreType.DMA((seq,)),
        ],
        compiler_params=pltpu.CompilerParams(collective_id=0, has_side_effects=True),
        name="gather_keys",
    )(packed, queries, route)


def stick_kernel(seq, heads, head_size, bias_rows, query_ref, far_ref, every_ref, out_ref,
                 lhs, after, carried, total):
    me = lax.axis_index("sp")
    half = far_ref.shape[0]
    keys = every_ref.shape[2]
    depth = head_size + bias_rows
    scale = head_size ** (-0.5) * LOG2E
    keep_start = jnp.where(me < seq // 2, 0, half)
    row_id = lax.broadcasted_iota(jnp.int32, (keys, keys), 0)
    col_id = lax.broadcasted_iota(jnp.int32, (keys, keys), 1)
    after[...] = jnp.where(row_id > col_id, 1.0, 0.0).astype(jnp.bfloat16)
    group = HEADS_AT_ONCE
    rows = group * half
    mark = lax.broadcasted_iota(jnp.int32, (half, bias_rows), 1)
    for part in range(2):
        for head in range(heads):
            columns = slice(head * head_size, (head + 1) * head_size)
            if part == 0:
                mine = query_ref[pl.ds(pl.multiple_of(keep_start, half), half), columns]
            else:
                mine = far_ref[:, columns]
            at = pl.ds(head * half, half)
            lhs[at, 0:head_size] = mine
            lhs[at, head_size:depth] = jnp.where(mark == head, 1.0, 0.0).astype(jnp.bfloat16)
        owner = me if part == 0 else seq - 1 - me

        def sweep(block, diagonal):
            for turn in range(heads // group):
                at = pl.ds(turn * rows, rows)
                logits = (
                    jnp.dot(
                        lhs[at, :],
                        every_ref[block, 0:depth, :],
                        preferred_element_type=jnp.float32,
                    )
                    * scale
                )
                soft = jnp.maximum(logits, 0.0) + jnp.log2(1.0 + jnp.exp2(-jnp.abs(logits)))
                take = logits - soft
                if diagonal:
                    row = lax.broadcasted_iota(jnp.int32, (rows, keys), 0) % half + keep_start
                    valid = lax.broadcasted_iota(jnp.int32, (rows, keys), 1) < row
                    soft = jnp.where(valid, soft, 0.0)
                beyond = jnp.dot(
                    soft.astype(jnp.bfloat16), after[...], preferred_element_type=jnp.float32
                )
                if diagonal:
                    weight = jnp.where(valid, jnp.exp2(take - beyond), 0.0)
                else:
                    weight = jnp.exp2(take - (beyond + carried[at, :]))
                product = lax.dot_general(
                    weight.astype(jnp.bfloat16),
                    every_ref[block, depth : depth + head_size, :],
                    (((1,), (1,)), ((), ())),
                    preferred_element_type=jnp.float32,
                )
                here = beyond[:, 0:1] + soft[:, 0:1]
                if diagonal:
                    total[at, :] = product
                    carried[at, :] = here
                else:
                    total[at, :] += product
                    carried[at, :] += here

        sweep(owner, True)

        @pl.loop(0, owner)
        def _(step):
            sweep(owner - 1 - step, False)

        for head in range(heads):
            out_ref[part * half : (part + 1) * half, head * head_size : (head + 1) * head_size] = (
                total[head * half : (head + 1) * half, :].astype(jnp.bfloat16)
            )


def stick_attention(queries, far, every, heads, head_size, bias_rows):
    vmem = pl.BlockSpec(memory_space=pltpu.VMEM)
    seq, _, keys = every.shape
    half = far.shape[0]
    elements = 9 * heads * half * keys
    return pl.pallas_call(
        functools.partial(stick_kernel, seq, heads, head_size, bias_rows),
        out_shape=jax.ShapeDtypeStruct(queries.shape, queries.dtype),
        in_specs=[vmem] * 3,
        out_specs=vmem,
        scratch_shapes=[
            pltpu.VMEM((heads * half, head_size + bias_rows), jnp.bfloat16),
            pltpu.VMEM((keys, keys), jnp.bfloat16),
            pltpu.VMEM((heads * half, 1), jnp.float32),
            pltpu.VMEM((heads * half, head_size), jnp.float32),
        ],
        cost_estimate=pl.CostEstimate(
            flops=2 * elements * (keys + 2 * head_size),
            bytes_accessed=2 * every.size,
            transcendentals=3 * elements,
        ),
        name="stick_attention",
    )(queries, far, every)


def owners_kernel(seq, ranks, part_ref, out_ref, send, recv, local):
    me, rank = lax.axis_index("sp"), lax.axis_index("tp")
    mirror = seq - 1 - me
    chunk = out_ref.shape[0]
    width = part_ref.shape[1]
    barrier = pltpu.get_barrier_semaphore()
    for step in range(1, ranks):
        pl.semaphore_signal(
            barrier,
            inc=1,
            device_id={"sp": me, "tp": (rank + step) % ranks},
            device_id_type=MESH,
        )
    for step in range(ranks):
        pl.semaphore_signal(
            barrier, inc=1, device_id={"sp": mirror, "tp": step}, device_id_type=MESH
        )
    pl.semaphore_wait(barrier, 2 * ranks - 1)
    half = ranks // 2
    first = jnp.where(me < seq // 2, 0, half)
    place = pl.ds(pl.multiple_of(rank * width, width), width)

    def push(index, owner, target):
        return pltpu.make_async_remote_copy(
            src_ref=part_ref.at[pl.ds(index * chunk, chunk)],
            dst_ref=out_ref.at[:, place],
            send_sem=send.at[index],
            recv_sem=recv.at[rank],
            device_id={"sp": owner, "tp": target},
            device_id_type=MESH,
        )

    def stays(index):
        return pltpu.make_async_copy(
            part_ref.at[pl.ds(index * chunk, chunk)], out_ref.at[:, place], local
        )

    for index in range(half, ranks):
        push(index, mirror, first + index - half).start()
    for index in range(half):
        target = first + index

        @pl.when(target != rank)
        def _():
            push(index, me, target).start()

        @pl.when(target == rank)
        def _():
            stays(index).start()

    kept = (rank // half) * half == first

    for source in range(ranks):

        @pl.when(jnp.logical_not(jnp.logical_and(kept, rank == source)))
        def _():
            pltpu.make_async_remote_copy(
                src_ref=part_ref.at[pl.ds(0, chunk)],
                dst_ref=out_ref.at[:, source * width : (source + 1) * width],
                send_sem=send.at[0],
                recv_sem=recv.at[source],
                device_id={"sp": mirror, "tp": source},
                device_id_type=MESH,
            ).wait_recv()

    for index in range(half, ranks):
        push(index, mirror, first + index - half).wait_send()
    for index in range(half):
        target = first + index

        @pl.when(target != rank)
        def _():
            push(index, me, target).wait_send()

        @pl.when(target == rank)
        def _():
            stays(index).wait()


def to_owners(part, seq, ranks):
    vmem = pl.BlockSpec(memory_space=pltpu.VMEM)
    rows, width = part.shape
    return pl.pallas_call(
        functools.partial(owners_kernel, seq, ranks),
        out_shape=jax.ShapeDtypeStruct((rows // ranks, width * ranks), part.dtype),
        in_specs=[vmem],
        out_specs=vmem,
        scratch_shapes=[
            pltpu.SemaphoreType.DMA((ranks,)),
            pltpu.SemaphoreType.DMA((ranks,)),
            pltpu.SemaphoreType.DMA,
        ],
        compiler_params=pltpu.CompilerParams(collective_id=1, has_side_effects=True),
        name="to_owners",
    )(part)


def greet(seq, ranks, me, rank):
    barrier = pltpu.get_barrier_semaphore()
    for step in range(1, seq):
        pl.semaphore_signal(
            barrier, inc=1, device_id={"sp": (me + step) % seq}, device_id_type=MESH
        )
    for step in range(1, ranks):
        pl.semaphore_signal(
            barrier, inc=1, device_id={"tp": (rank + step) % ranks}, device_id_type=MESH
        )
    pl.semaphore_wait(barrier, seq + ranks - 2)


def dispatch_kernel(seq, ranks, rows_ref, pick_ref, out_ref, every, stage, send, recv, t_send,
                    t_recv):
    me, rank = lax.axis_index("sp"), lax.axis_index("tp")
    partner = me + 1 - 2 * (me % 2)
    capacity, width = out_ref.shape[2:]
    greet(seq, ranks, me, rank)

    def push(source, block, target, slot):
        return pltpu.make_async_remote_copy(
            src_ref=source,
            dst_ref=every.at[block],
            send_sem=send.at[slot],
            recv_sem=recv.at[block],
            device_id={"sp": target},
            device_id_type=MESH,
        )

    def hand(block, step):
        target = (rank + step) % ranks
        return pltpu.make_async_remote_copy(
            src_ref=stage.at[block, target],
            dst_ref=out_ref.at[rank, block],
            send_sem=t_send.at[block, step],
            recv_sem=t_recv.at[rank],
            device_id={"tp": target},
            device_id_type=MESH,
        )

    def pack(block, source):
        for start in range(0, width, 512):
            columns = slice(start, start + 512)
            packed = jnp.dot(
                pick_ref[block], source[:, columns], preferred_element_type=jnp.float32
            ).astype(jnp.bfloat16)
            for target in range(ranks):
                stage[block, target, :, columns] = packed[
                    target * capacity : (target + 1) * capacity
                ]
        for step in range(1, ranks):
            hand(block, step).start()
        out_ref[rank, block] = stage[block, rank]

    steps = seq // 2
    sent = [push(rows_ref, me, partner, 0)]
    for step in range(1, steps):
        sent.append(push(rows_ref, me, (me + 2 * step) % seq, step))
    for copy in sent:
        copy.start()
    pack(me, rows_ref)
    for step in range(steps):
        if step:
            block = (me + seq - 2 * step) % seq
            copy = push(every.at[block], block, partner, steps + step)
            push(rows_ref, block, partner, 0).wait_recv()
            copy.start()
            sent.append(copy)
            pack(block, every.at[block])
        block = (partner + seq - 2 * step) % seq
        push(rows_ref, block, partner, 0).wait_recv()
        pack(block, every.at[block])
    for step in range(1, ranks):
        source = (rank + step) % ranks
        pltpu.make_async_remote_copy(
            src_ref=out_ref.at[source],
            dst_ref=out_ref.at[source],
            send_sem=t_send.at[0, 0],
            recv_sem=t_recv.at[source],
            device_id={"tp": source},
            device_id_type=MESH,
        ).wait_recv()
    for copy in sent:
        copy.wait_send()
    for block in range(seq):
        for step in range(1, ranks):
            hand(block, step).wait_send()


def dispatch(rows, pick, seq, ranks, capacity):
    vmem = pl.BlockSpec(memory_space=pltpu.VMEM)
    width = rows.shape[1]
    return pl.pallas_call(
        functools.partial(dispatch_kernel, seq, ranks),
        out_shape=jax.ShapeDtypeStruct((ranks, seq, capacity, width), rows.dtype),
        in_specs=[vmem] * 2,
        out_specs=vmem,
        scratch_shapes=[
            pltpu.VMEM((seq,) + rows.shape, rows.dtype),
            pltpu.VMEM((seq, ranks, capacity, width), rows.dtype),
            pltpu.SemaphoreType.DMA((seq,)),
            pltpu.SemaphoreType.DMA((seq,)),
            pltpu.SemaphoreType.DMA((seq, ranks)),
            pltpu.SemaphoreType.DMA((ranks,)),
        ],
        compiler_params=pltpu.CompilerParams(collective_id=2, has_side_effects=True),
        name="dispatch",
    )(rows, pick)


def combine_kernel(seq, ranks, done_ref, gate_ref, out_ref, back, lent, landed, finished, arrived,
                   t_send, t_recv, y_send, y_recv, z_send, z_recv):
    me, rank = lax.axis_index("sp"), lax.axis_index("tp")
    partner = me + 1 - 2 * (me % 2)
    capacity, width = done_ref.shape[2:]
    steps = seq // 2
    slots = ranks * capacity
    greet(seq, ranks, me, rank)

    def hand(block, step):
        target = (rank + step) % ranks
        return pltpu.make_async_remote_copy(
            src_ref=done_ref.at[target, block],
            dst_ref=back.at[block, rank],
            send_sem=t_send.at[block, step],
            recv_sem=t_recv.at[block],
            device_id={"tp": target},
            device_id_type=MESH,
        )

    def lend(block, step):
        return pltpu.make_async_remote_copy(
            src_ref=lent.at[step],
            dst_ref=landed.at[step],
            send_sem=y_send.at[step],
            recv_sem=y_recv.at[step],
            device_id={"sp": partner},
            device_id_type=MESH,
        )

    def give(step):
        return pltpu.make_async_remote_copy(
            src_ref=finished.at[step],
            dst_ref=arrived.at[step],
            send_sem=z_send.at[step],
            recv_sem=z_recv.at[step],
            device_id={"sp": (me + 2 * step) % seq},
            device_id_type=MESH,
        )

    order = list(range(1, steps)) + [0]
    for turn in order:
        for base in (partner, me):
            block = (base + 2 * turn) % seq
            for step in range(1, ranks):
                hand(block, step).start()
            back[block, rank] = done_ref[rank, block]

    def await_back(block):
        pltpu.make_async_remote_copy(
            src_ref=back.at[block, pl.ds(0, ranks - 1)],
            dst_ref=back.at[block, pl.ds(0, ranks - 1)],
            send_sem=t_send.at[block, 0],
            recv_sem=t_recv.at[block],
            device_id={"sp": partner},
            device_id_type=MESH,
        ).wait_recv()

    def weighted(block, columns):
        rows = jnp.concatenate([back[block, t, :, columns] for t in range(ranks)], axis=0)
        return jnp.dot(
            gate_ref[block, :, 0:slots], rows, preferred_element_type=jnp.float32
        ) + jnp.dot(gate_ref[block, :, slots:], rows, preferred_element_type=jnp.float32)

    for turn in order:
        block = (partner + 2 * turn) % seq
        await_back(block)
        for start in range(0, width, 512):
            columns = slice(start, start + 512)
            lent[turn, :, columns] = weighted(block, columns).astype(jnp.bfloat16)
        lend(block, turn).start()
        block = (me + 2 * turn) % seq
        await_back(block)
        lend(block, turn).wait_recv()
        for start in range(0, width, 512):
            columns = slice(start, start + 512)
            here = weighted(block, columns) + landed[turn, :, columns].astype(jnp.float32)
            if turn:
                finished[turn, :, columns] = here.astype(jnp.bfloat16)
            else:
                out_ref[:, columns] = here
        if turn:
            give(turn).start()
    for turn in range(1, steps):
        give(turn).wait_recv()
        out_ref[...] += arrived[turn].astype(jnp.float32)
    for turn in range(steps):
        lend(me, turn).wait_send()
        if turn:
            give(turn).wait_send()
    for block in range(seq):
        for step in range(1, ranks):
            hand(block, step).wait_send()


def combine(done, gate, seq, ranks):
    vmem = pl.BlockSpec(memory_space=pltpu.VMEM)
    capacity, width = done.shape[2:]
    rows = gate.shape[1]
    steps = seq // 2
    return pl.pallas_call(
        functools.partial(combine_kernel, seq, ranks),
        out_shape=jax.ShapeDtypeStruct((rows, width), jnp.float32),
        in_specs=[vmem] * 2,
        out_specs=vmem,
        scratch_shapes=[pltpu.VMEM((seq, ranks, capacity, width), done.dtype)]
        + [pltpu.VMEM((steps, rows, width), done.dtype)] * 4
        + [
            pltpu.SemaphoreType.DMA((seq, ranks)),
            pltpu.SemaphoreType.DMA((seq,)),
        ]
        + [pltpu.SemaphoreType.DMA((steps,))] * 4,
        compiler_params=pltpu.CompilerParams(collective_id=3, has_side_effects=True),
        name="combine",
    )(done, gate)


def expert_rows(arrived, w_gate, w_up, w_down):
    gate_part = jnp.einsum("nd,df->nf", arrived, w_gate, preferred_element_type=jnp.float32)
    up_part = jnp.einsum("nd,df->nf", arrived, w_up, preferred_element_type=jnp.float32)
    inner = (jax.nn.silu(gate_part) * up_part).astype(jnp.bfloat16)
    return jnp.einsum("nf,fd->nd", inner, w_down, preferred_element_type=jnp.float32).astype(
        jnp.bfloat16
    )


def body(
    queries,
    key_value,
    break_bias,
    stream,
    out_proj,
    ffn_gain,
    routes,
    route_score,
    expert_gate,
    expert_up,
    expert_down,
    shared_gate,
    shared_up,
    shared_down,
):
    kv_local = key_value.shape[1]
    head_size = key_value.shape[2] // 2
    group_size = break_bias.shape[1] // kv_local
    bias_rows = -(-group_size // 16) * 16
    shift = (break_bias.astype(jnp.float32) * head_size**0.5).astype(jnp.bfloat16)
    joined = key_value[:, 0, :].T
    packed = jnp.concatenate(
        [
            joined[:head_size],
            jnp.pad(shift.T, ((0, bias_rows - group_size), (0, 0))),
            joined[head_size:],
        ],
        axis=0,
    )
    gates = 2.5 * route_score / jnp.sum(route_score, axis=1, keepdims=True)
    row_count, top_count = routes.shape
    seq_count = lax.axis_size("sp")
    rank_count = lax.axis_size("tp")
    expert_count = seq_count * rank_count
    capacity = 2 * row_count * top_count // expert_count
    flat_expert = routes.reshape(-1)
    onehot = (flat_expert[:, None] == jnp.arange(expert_count, dtype=jnp.int32)[None, :]).astype(
        jnp.int32
    )
    rank = jnp.sum((jnp.cumsum(onehot, axis=0) - onehot) * onehot, axis=1)
    slot_ids = (flat_expert * capacity + rank).reshape(row_count, top_count)
    route_plan = jnp.concatenate([slot_ids.astype(jnp.float32).T, gates.T], axis=0)
    every, far, plans = gather_keys(packed, queries, route_plan, seq_count)
    group_slots = rank_count * capacity
    near = (
        plans[:, :top_count].astype(jnp.int32) - lax.axis_index("sp") * group_slots
    )
    slot_grid = jnp.arange(group_slots, dtype=jnp.int32)
    pick = jnp.any(near[:, :, None, :] == slot_grid[None, None, :, None], axis=1).astype(
        jnp.bfloat16
    )
    weight = jnp.sum(
        jnp.where(
            near[:, :, :, None] == slot_grid[None, None, None, :],
            plans[:, top_count:, :, None],
            0.0,
        ),
        axis=1,
    )
    coarse = weight.astype(jnp.bfloat16)
    fine = (weight - coarse.astype(jnp.float32)).astype(jnp.bfloat16)
    gate_grid = jnp.concatenate([coarse, fine], axis=2)
    attended = stick_attention(queries, far, every, group_size, head_size, bias_rows)
    token_heads = to_owners(attended, seq_count, rank_count)
    mixed = jnp.dot(token_heads, out_proj, preferred_element_type=jnp.float32)
    resid = (stream.astype(jnp.float32) + mixed).astype(jnp.bfloat16)
    wide = resid.astype(jnp.float32)
    factor = lax.rsqrt(jnp.mean(wide * wide, axis=-1, keepdims=True) + 1e-06)
    normed = (wide * factor * ffn_gain).astype(jnp.bfloat16)
    arrived = dispatch(normed, pick, seq_count, rank_count, capacity)
    done = expert_rows(
        arrived.reshape(-1, arrived.shape[-1]), expert_gate[0], expert_up[0], expert_down[0]
    )
    routed = combine(done.reshape(arrived.shape), gate_grid, seq_count, rank_count)
    shared_inner = (
        jax.nn.silu(jnp.dot(normed, shared_gate, preferred_element_type=jnp.float32))
        * jnp.dot(normed, shared_up, preferred_element_type=jnp.float32)
    ).astype(jnp.bfloat16)
    shared_out = jnp.dot(shared_inner, shared_down, preferred_element_type=jnp.float32)
    return (wide + shared_out + routed).astype(jnp.bfloat16)


def solution(mesh):
    return jax.shard_map(
        body,
        mesh=mesh,
        in_specs=(
            P("sp", "tp"),
            P("sp", "tp", None),
            P("sp", "tp"),
            P(("sp", "tp"), None),
            P(),
            P(),
            P(("sp", "tp"), None),
            P(("sp", "tp"), None),
            P(("sp", "tp"), None, None),
            P(("sp", "tp"), None, None),
            P(("sp", "tp"), None, None),
            P(),
            P(),
            P(),
        ),
        out_specs=P(("sp", "tp"), None),
        check_vma=False,
    )
```

profile of v0, /device:TPU:25, one launch (start us, length us, event | category | flops | bytes accessed | tf_op | source)
XLA Modules:
  0.0 169.3 jit_solution(9239050389487012457)
XLA Ops:
  0.0 0.9 copy.22
  0.9 0.1 eq.55
  1.0 0.6 reduce-window.6
  1.6 0.2 slice_reduce_fusion
  1.9 0.1 eq.51
  2.0 0.1 fusion.32
  2.1 0.1 reduce_sum.39
  2.2 0.1 copy.25
  2.3 0.7 convert_bitcast_fusion
  3.0 0.7 reduce_sum.40
  3.7 0.7 divide_bitcast_fusion
  4.3 0.6 pad_maximum_fusion.1.route_ref
  4.9 0.9 copy.21
  5.9 0.7 fusion.34
  6.6 0.6 fusion.28.packed_ref
  7.2 17.8 %gather_keys.1 = (bf16[8,144,256]{2,1,0:T(8,128)(2,1)}, bf16[128,512]{1,0:T(8,128)(2,1)}, f32[8,8,64]{2,1,0:T(8,128)}) custom-call(bf16[144,256]{1,0:T(8,128)(2,1)} %fusion.28.packed_ref, bf16[256,512]{1,0:T(8,128)(2,1)} %query_ref.3, f32[8,64]{1,0:T(8,128)} %pad_maximum_fusion.1.route_ref), custom_call_target="tpu_custom_call" | custom-call | tf_op jit(solution)/shard_map/gather_keys/pallas_call | solution.py:100
  25.1 0.0 copy-start.3
  25.1 10.4 %stick_attention.1.part_ref = bf16[256,512]{1,0:T(8,128)(2,1)} custom-call(bf16[256,512]{1,0:T(8,128)(2,1)} %query_ref.3, bf16[128,512]{1,0:T(8,128)(2,1)} %get-tuple-element.8.far_ref, bf16[8,144,256]{2,1,0:T(8,128)(2,1)} %get-tuple-element.9.every_ref), custom_call_target="tpu_custom_call" | custom-call | flops 1811939328 | bytes 589824 | tf_op jit(solution)/shard_map/stick_attention/pallas_call | solution.py:203
  35.4 16.9 %to_owners.1 = bf16[64,2048]{1,0:T(8,128)(2,1)} custom-call(bf16[256,512]{1,0:T(8,128)(2,1)} %stick_attention.1.part_ref), custom_call_target="tpu_custom_call" | custom-call | tf_op jit(solution)/shard_map/to_owners/pallas_call | solution.py:305
  52.3 0.0 copy-start.5
  52.4 5.2 %multiply_reduce_fusion = (f32[64]{0:T(128)S(1)}, f32[64,2048]{1,0:T(8,128)S(1)}) fusion(bf16[64,2048]{1,0:T(8,128)(2,1)} %to_owners.1, bf16[2048,2048]{1,0:T(8,128)(2,1)} %param.18, bf16[64,2048]{1,0:T(8,128)(2,1)S(1)} %copy-done.3), kind=kOutput, calls=%fused_computation.22 | convolution fusion | flops 537657280 | bytes 9437440 | tf_op jit(solution)/shard_map/dot_general | solution.py:622
  57.6 0.8 multiply_convert_fusion.rows_ref
  58.4 0.2 fusion.16
  58.6 0.7 convert_element_type.68.pick_ref
  59.3 45.9 %dispatch.1 = bf16[4,8,16,2048]{3,2,1,0:T(8,128)(2,1)} custom-call(bf16[64,2048]{1,0:T(8,128)(2,1)} %multiply_convert_fusion.rows_ref, bf16[8,64,64]{2,1,0:T(8,128)(2,1)} %convert_element_type.68.pick_ref), custom_call_target="tpu_custom_call" | custom-call | tf_op jit(solution)/shard_map/dispatch/pallas_call | solution.py:413
  105.2 4.5 %fusion.7 = f32[512,512]{1,0:T(8,128)} fusion(bf16[512,2048]{1,0:T(8,128)(2,1)} %bitcast.54, bf16[1,2048,512]{2,1,0:T(8,128)(2,1)} %param.22), kind=kOutput, calls=%fused_computation.10 | convolution fusion | flops 1073741824 | bytes 5242880 | tf_op jit(solution)/shard_map/nd,df->nf/dot_general | solution.py:549
  109.7 6.3 %convolution_convert_fusion = bf16[512,2048]{1,0:T(8,128)(2,1)} fusion(bf16[1,512,2048]{2,1,0:T(8,128)(2,1)S(1)} %copy-done, bf16[512,2048]{1,0:T(8,128)(2,1)} %bitcast.55, bf16[1,2048,512]{2,1,0:T(8,128)(2,1)} %param.23, f32[512,512]{1,0:T(8,128)} %fusion.7), kind=kOutput, calls=%fused_computation | convolution fusion | flops 2150105088 | bytes 9437184 | tf_op jit(solution)/shard_map/nf,fd->nd/dot_general | solution.py:552
  115.9 0.7 select_reduce_fusion
  116.7 0.8 pad_maximum_fusion.gate_ref
  117.5 45.8 %combine.1 = f32[64,2048]{1,0:T(8,128)} custom-call(bf16[4,8,16,2048]{3,2,1,0:T(8,128)(2,1)} %bitcast.56, bf16[8,64,128]{2,1,0:T(8,128)(2,1)} %pad_maximum_fusion.gate_ref), custom_call_target="tpu_custom_call" | custom-call | tf_op jit(solution)/shard_map/combine/pallas_call | solution.py:531
  163.3 2.1 %fusion.38 = f32[64,512]{1,0:T(8,128)S(1)} fusion(bf16[64,2048]{1,0:T(8,128)(2,1)S(1)} %copy-done.1, bf16[2048,512]{1,0:T(8,128)(2,1)} %param.25), kind=kOutput, calls=%fused_computation.56 | convolution fusion | flops 134217728 | bytes 2490368 | tf_op jit(solution)/shard_map/dot_general | solution.py:633
  165.4 3.8 %fusion.1 = bf16[64,2048]{1,0:T(8,128)(2,1)} fusion(f32[64,2048]{1,0:T(8,128)S(1)} %copy-done.2, f32[64,2048]{1,0:T(8,128)S(1)} %get-tuple-element.16, bf16[512,2048]{1,0:T(8,128)(2,1)} %param.27, bf16[64,2048]{1,0:T(8,128)(2,1)S(1)} %copy-done.1, bf16[2048,512]{1,0:T(8,128)(2,1)} %param.26, f32[64,512]{1,0:T(8,128)S(1)} %fusion.38), kind=kOutput, calls=%fused_computation.4 | convolution fusion | flops 269025280 | bytes 5898240 | tf_op jit(solution)/shard_map/dot_general | solution.py:636
  (18 shorter events, 0.1 us)
Async XLA Ops:
  0.0 109.7 %copy-start = (bf16[1,512,2048]{2,1,0:T(8,128)(2,1)S(1)}, bf16[1,512,2048]{2,1,0:T(8,128)(2,1)}, u32[]{:S(2)}) copy-start(bf16[1,512,2048]{2,1,0:T(8,128)(2,1)} %param.24) | copy-start | bytes 6291460
  25.1 27.3 %copy-start.3 = (bf16[64,2048]{1,0:T(8,128)(2,1)S(1)}, bf16[64,2048]{1,0:T(8,128)(2,1)}, u32[]{:S(2)}) copy-start(bf16[64,2048]{1,0:T(8,128)(2,1)} %param.17) | copy-start | bytes 786436
  52.3 5.2 %copy-start.5 = (f32[2048]{0:T(1024)S(1)}, f32[2048]{0:T(1024)}, u32[]{:S(2)}) copy-start(f32[2048]{0:T(1024)} %param.19) | copy-start | bytes 24580
  52.4 6.0 %copy-start.4 = (f32[8,8,64]{2,1,0:T(8,128)S(1)}, f32[8,8,64]{2,1,0:T(8,128)}, u32[]{:S(2)}) copy-start(f32[8,8,64]{2,1,0:T(8,128)} %get-tuple-element.10) | copy-start | bytes 49156
  115.9 47.4 %copy-start.1 = (bf16[64,2048]{1,0:T(8,128)(2,1)S(1)}, bf16[64,2048]{1,0:T(8,128)(2,1)}, u32[]{:S(2)}) copy-start(bf16[64,2048]{1,0:T(8,128)(2,1)} %multiply_convert_fusion.rows_ref) | copy-start | bytes 786436
  163.3 2.1 %copy-start.2 = (f32[64,2048]{1,0:T(8,128)S(1)}, f32[64,2048]{1,0:T(8,128)}, u32[]{:S(2)}) copy-start(f32[64,2048]{1,0:T(8,128)} %combine.1) | copy-start | bytes 1572868
where the time goes:
time: 172 us; the launch traced here: 169 us
  Pallas kernels  137 us (80%)
  matrix products  21.9 us (13%)
  other arithmetic  7.93 us (5%)
  local copies, waits for them, and re-layouts  2.48 us (1%)
    pallas_call x1, Pallas kernels, dispatch(): pl.pallas_call(functools.partial(dispatch_kernel, seq, ranks), out_shape=...  45.9 us
    pallas_call x1, Pallas kernels, combine(): pl.pallas_call(functools.partial(combine_kernel, seq, ranks), out_shape=j...  45.8 us
    pallas_call x1, Pallas kernels, gather_keys(): pl.pallas_call(functools.partial(gather_kernel, seq, half), out_shape=(ja...  17.8 us
    pallas_call x1, Pallas kernels, to_owners(): pl.pallas_call(functools.partial(owners_kernel, seq, ranks), out_shape=ja...  16.9 us
    pallas_call x1, Pallas kernels, stick_attention(): pl.pallas_call(functools.partial(stick_kernel, seq, heads, head_size, bia...  10.4 us
    dot_general x1, matrix products, expert_rows(): jnp.einsum('nf,fd->nd', inner, w_down, preferred_element_type=jnp.float32)  6.27 us
    dot_general x1, matrix products, body(): mixed = jnp.dot(token_heads, out_proj, preferred_element_type=jnp.float32)  5.18 us
    dot_general x1, matrix products, expert_rows(): jnp.einsum('nd,df->nf', arrived, w_gate, preferred_element_type=jnp.float32)  4.45 us

commit v1 on v0

--- a/solution.py
+++ b/solution.py
@@ -317,241 +317,331 @@
     )(part)
 
 
-def greet(seq, ranks, me, rank):
+def moe_kernel(seq, ranks, top, cap, resid_ref, gain_ref, plans_ref, gate_hbm, up_hbm, down_hbm,
+               s_gate_hbm, s_up_hbm, s_down_hbm, out_ref, w_gate, w_up, w_down, v_gate, v_up,
+               v_down, rows, stage, arrived, done, back, part, land, base, inner, loads, z_send,
+               z_recv, d_send, d_recv, b_send, b_recv, l_send, l_recv):
+    me, rank = lax.axis_index("sp"), lax.axis_index("tp")
+    line = seq // 2
+    z, y = me // 2, me % 2
+    plane = 2 * ranks
+    mine = y * ranks + rank
+    count, width = resid_ref.shape
+    slots = plane * cap
+    piece = width // l_send.shape[1]
     barrier = pltpu.get_barrier_semaphore()
-    for step in range(1, seq):
+    for step in range(1, plane):
+        other = (mine + step) % plane
         pl.semaphore_signal(
-            barrier, inc=1, device_id={"sp": (me + step) % seq}, device_id_type=MESH
-        )
-    for step in range(1, ranks):
-        pl.semaphore_signal(
-            barrier, inc=1, device_id={"tp": (rank + step) % ranks}, device_id_type=MESH
-        )
-    pl.semaphore_wait(barrier, seq + ranks - 2)
-
-
-def dispatch_kernel(seq, ranks, rows_ref, pick_ref, out_ref, every, stage, send, recv, t_send,
-                    t_recv):
-    me, rank = lax.axis_index("sp"), lax.axis_index("tp")
-    partner = me + 1 - 2 * (me % 2)
-    capacity, width = out_ref.shape[2:]
-    greet(seq, ranks, me, rank)
-
-    def push(source, block, target, slot):
+            barrier,
+            inc=1,
+            device_id={"sp": 2 * z + other // ranks, "tp": other % ranks},
+            device_id_type=MESH,
+        )
+
+    @pl.when(z > 0)
+    def _():
+        pl.semaphore_signal(barrier, inc=1, device_id={"sp": me - 2}, device_id_type=MESH)
+
+    @pl.when(z < line - 1)
+    def _():
+        pl.semaphore_signal(barrier, inc=1, device_id={"sp": me + 2}, device_id_type=MESH)
+
+    pairs = [
+        (s_gate_hbm, v_gate),
+        (s_up_hbm, v_up),
+        (s_down_hbm, v_down),
+        (gate_hbm, w_gate),
+        (up_hbm, w_up),
+        (down_hbm, w_down),
+    ]
+    fetches = [
+        pltpu.make_async_copy(source, target, loads.at[index])
+        for index, (source, target) in enumerate(pairs)
+    ]
+    for fetch in fetches:
+        fetch.start()
+
+    wide = resid_ref[...].astype(jnp.float32)
+    factor = lax.rsqrt(jnp.mean(wide * wide, axis=-1, keepdims=True) + 1e-06)
+    rows[z] = (wide * factor * gain_ref[...]).astype(jnp.bfloat16)
+    pl.semaphore_wait(
+        barrier,
+        plane - 1 + jnp.where(z > 0, 1, 0) + jnp.where(z < line - 1, 1, 0),
+    )
+
+    def block_at(k):
+        low, high = z, line - 1 - z
+        both = jnp.minimum(low, high)
+        near = jnp.where(k % 2 == 1, z + (k + 1) // 2, z - (k + 1) // 2)
+        far = jnp.where(low > high, z - (k - both), z + (k - both))
+        return jnp.where(k <= 2 * both, near, far)
+
+    def shift(block, way):
         return pltpu.make_async_remote_copy(
-            src_ref=source,
-            dst_ref=every.at[block],
-            send_sem=send.at[slot],
-            recv_sem=recv.at[block],
-            device_id={"sp": target},
-            device_id_type=MESH,
-        )
-
-    def hand(block, step):
-        target = (rank + step) % ranks
+            src_ref=rows.at[block],
+            dst_ref=rows.at[block],
+            send_sem=z_send.at[block, (way + 1) // 2],
+            recv_sem=z_recv.at[block],
+            device_id={"sp": me + 2 * way},
+            device_id_type=MESH,
+        )
+
+    def inside(block, way):
+        low = z - 1 >= 0 if way < 0 else z + 1 < line
+        return jnp.logical_and(low, block >= z if way < 0 else block <= z)
+
+    def forward(block, act):
+        for way in (-1, 1):
+
+            @pl.when(inside(block, way))
+            def _(way=way):
+                act(shift(block, way))
+
+    def hand(source, target, block, step, sends, recvs):
+        other = (mine + step) % plane
         return pltpu.make_async_remote_copy(
-            src_ref=stage.at[block, target],
-            dst_ref=out_ref.at[rank, block],
-            send_sem=t_send.at[block, step],
-            recv_sem=t_recv.at[rank],
-            device_id={"tp": target},
-            device_id_type=MESH,
-        )
-
-    def pack(block, source):
+            src_ref=source.at[block, other],
+            dst_ref=target.at[block, mine],
+            send_sem=sends.at[block, step],
+            recv_sem=recvs.at[block],
+            device_id={"sp": 2 * z + other // ranks, "tp": other % ranks},
+            device_id_type=MESH,
+        )
+
+    def gathered(target, block, recvs):
+        return pltpu.make_async_remote_copy(
+            src_ref=target.at[block, pl.ds(0, plane - 1)],
+            dst_ref=target.at[block, pl.ds(0, plane - 1)],
+            send_sem=z_send.at[0, 0],
+            recv_sem=recvs.at[block],
+            device_id={"tp": (rank + 1) % ranks},
+            device_id_type=MESH,
+        )
+
+    def slot_grid(block):
+        plan = plans_ref[2 * block + y]
+        spots = lax.broadcasted_iota(jnp.int32, (slots, count), 0) + z * slots
+        return plan, spots
+
+    def send_rows(block):
+        plan, spots = slot_grid(block)
+        hit = None
+        for k in range(top):
+            same = plan[k : k + 1, :].astype(jnp.int32) == spots
+            hit = same if hit is None else jnp.logical_or(hit, same)
+        pick = jnp.where(hit, 1.0, 0.0).astype(jnp.bfloat16)
         for start in range(0, width, 512):
             columns = slice(start, start + 512)
             packed = jnp.dot(
-                pick_ref[block], source[:, columns], preferred_element_type=jnp.float32
+                pick, rows[block, :, columns], preferred_element_type=jnp.float32
             ).astype(jnp.bfloat16)
-            for target in range(ranks):
-                stage[block, target, :, columns] = packed[
-                    target * capacity : (target + 1) * capacity
-                ]
-        for step in range(1, ranks):
-            hand(block, step).start()
-        out_ref[rank, block] = stage[block, rank]
-
-    steps = seq // 2
-    sent = [push(rows_ref, me, partner, 0)]
-    for step in range(1, steps):
-        sent.append(push(rows_ref, me, (me + 2 * step) % seq, step))
-    for copy in sent:
-        copy.start()
-    pack(me, rows_ref)
-    for step in range(steps):
-        if step:
-            block = (me + seq - 2 * step) % seq
-            copy = push(every.at[block], block, partner, steps + step)
-            push(rows_ref, block, partner, 0).wait_recv()
-            copy.start()
-            sent.append(copy)
-            pack(block, every.at[block])
-        block = (partner + seq - 2 * step) % seq
-        push(rows_ref, block, partner, 0).wait_recv()
-        pack(block, every.at[block])
-    for step in range(1, ranks):
-        source = (rank + step) % ranks
+            for other in range(plane):
+                stage[block, other, :, columns] = packed[other * cap : (other + 1) * cap]
+        for step in range(1, plane):
+            hand(stage, arrived, block, step, d_send, d_recv).start()
+        arrived[block, mine] = stage[block, mine]
+
+    def join(source, block, columns=slice(None)):
+        return jnp.concatenate(
+            [source[block, other, :, columns] for other in range(plane)], axis=0
+        )
+
+    def expert(block):
+        gathered(arrived, block, d_recv).wait_recv()
+        taken = join(arrived, block)
+        hidden = w_gate.shape[1]
+        for start in range(0, hidden, 256):
+            columns = slice(start, start + 256)
+            gate = jnp.dot(taken, w_gate[:, columns], preferred_element_type=jnp.float32)
+            up = jnp.dot(taken, w_up[:, columns], preferred_element_type=jnp.float32)
+            inner[0:slots, columns] = (jax.nn.silu(gate) * up).astype(jnp.bfloat16)
+        for start in range(0, width, 512):
+            columns = slice(start, start + 512)
+            result = jnp.dot(
+                inner[0:slots, :], w_down[:, columns], preferred_element_type=jnp.float32
+            ).astype(jnp.bfloat16)
+            for other in range(plane):
+                done[block, other, :, columns] = result[other * cap : (other + 1) * cap]
+
+    def give_back(block):
+        for step in range(1, plane):
+            hand(done, back, block, step, b_send, b_recv).start()
+        back[block, mine] = done[block, mine]
+
+    def weights_of(block):
+        plan, spots = slot_grid(block)
+        total = jnp.zeros((slots, count), jnp.float32)
+        for k in range(top):
+            same = plan[k : k + 1, :].astype(jnp.int32) == spots
+            total = total + jnp.where(same, plan[top + k : top + k + 1, :], 0.0)
+        turned = total.T
+        coarse = turned.astype(jnp.bfloat16)
+        return coarse, (turned - coarse.astype(jnp.float32)).astype(jnp.bfloat16)
+
+    def summed(coarse, fine, block, columns):
+        taken = join(back, block, columns)
+        return jnp.dot(coarse, taken, preferred_element_type=jnp.float32) + jnp.dot(
+            fine, taken, preferred_element_type=jnp.float32
+        )
+
+    def pass_on(block, way, index):
+        target = z + way
+        slot = jnp.where(jnp.logical_and(way < 0, block == target), line, block)
+        at = pl.ds(index * piece, piece)
+        return pltpu.make_async_remote_copy(
+            src_ref=part.at[block, :, at],
+            dst_ref=land.at[slot, :, at],
+            send_sem=l_send.at[block, index],
+            recv_sem=l_recv.at[slot, index],
+            device_id={"sp": me + 2 * way},
+            device_id_type=MESH,
+        )
+
+    def landed(slot, index):
+        at = pl.ds(index * piece, piece)
+        return pltpu.make_async_remote_copy(
+            src_ref=land.at[slot, :, at],
+            dst_ref=land.at[slot, :, at],
+            send_sem=z_send.at[0, 0],
+            recv_sem=l_recv.at[slot, index],
+            device_id={"tp": (rank + 1) % ranks},
+            device_id_type=MESH,
+        )
+
+    pieces = [(index, slice(index * piece, (index + 1) * piece)) for index in range(width // piece)]
+
+    def collect(block):
+        way = jnp.where(block > z, 1, -1)
+        behind = jnp.where(block > z, z > 0, z < line - 1)
+        coarse, fine = weights_of(block)
+        gathered(back, block, b_recv).wait_recv()
+        for index, columns in pieces:
+            here = summed(coarse, fine, block, columns)
+
+            @pl.when(behind)
+            def _():
+                landed(block, index).wait_recv()
+                part[block, :, columns] = (
+                    here + land[block, :, columns].astype(jnp.float32)
+                ).astype(jnp.bfloat16)
+
+            @pl.when(jnp.logical_not(behind))
+            def _():
+                part[block, :, columns] = here.astype(jnp.bfloat16)
+
+            pass_on(block, way, index).start()
+
+    forward(z, lambda copy: copy.start())
+    send_rows(z)
+
+    for fetch in fetches[:3]:
+        fetch.wait()
+    normed = rows[z]
+    shared = v_gate.shape[1]
+    for start in range(0, shared, 256):
+        columns = slice(start, start + 256)
+        gate = jnp.dot(normed, v_gate[:, columns], preferred_element_type=jnp.float32)
+        up = jnp.dot(normed, v_up[:, columns], preferred_element_type=jnp.float32)
+        inner[0:count, columns] = (jax.nn.silu(gate) * up).astype(jnp.bfloat16)
+    for start in range(0, width, 512):
+        columns = slice(start, start + 512)
+        base[:, columns] = resid_ref[:, columns].astype(jnp.float32) + jnp.dot(
+            inner[0:count, :], v_down[:, columns], preferred_element_type=jnp.float32
+        )
+    for fetch in fetches[3:]:
+        fetch.wait()
+
+    @pl.loop(1, line)
+    def _(k):
+        block = block_at(k)
         pltpu.make_async_remote_copy(
-            src_ref=out_ref.at[source],
-            dst_ref=out_ref.at[source],
-            send_sem=t_send.at[0, 0],
-            recv_sem=t_recv.at[source],
-            device_id={"tp": source},
+            src_ref=rows.at[block],
+            dst_ref=rows.at[block],
+            send_sem=z_send.at[0, 0],
+            recv_sem=z_recv.at[block],
+            device_id={"tp": (rank + 1) % ranks},
             device_id_type=MESH,
         ).wait_recv()
-    for copy in sent:
-        copy.wait_send()
-    for block in range(seq):
-        for step in range(1, ranks):
-            hand(block, step).wait_send()
-
-
-def dispatch(rows, pick, seq, ranks, capacity):
+        forward(block, lambda copy: copy.start())
+        send_rows(block)
+        expert(block_at(k - 1))
+
+    expert(block_at(line - 1))
+
+    @pl.loop(0, line)
+    def _(k):
+        give_back(block_at(line - 1 - k))
+
+    @pl.loop(0, line - 1)
+    def _(k):
+        collect(block_at(line - 1 - k))
+
+    coarse, fine = weights_of(z)
+    gathered(back, z, b_recv).wait_recv()
+    for index, columns in pieces:
+        base[:, columns] += summed(coarse, fine, z, columns)
+
+    for index, columns in pieces:
+        for present, slot in ((z > 0, z), (z < line - 1, line)):
+
+            @pl.when(present)
+            def _(slot=slot):
+                landed(slot, index).wait_recv()
+                base[:, columns] += land[slot, :, columns].astype(jnp.float32)
+
+        out_ref[:, columns] = base[:, columns].astype(jnp.bfloat16)
+
+    @pl.loop(0, line)
+    def _(block):
+        forward(block, lambda copy: copy.wait_send())
+        for step in range(1, plane):
+            hand(stage, arrived, block, step, d_send, d_recv).wait_send()
+            hand(done, back, block, step, b_send, b_recv).wait_send()
+
+        @pl.when(block != z)
+        def _():
+            for index, _ in pieces:
+                pass_on(block, jnp.where(block > z, 1, -1), index).wait_send()
+
+
+def moe(resid, gain, plans, experts, shared, seq, ranks, top):
     vmem = pl.BlockSpec(memory_space=pltpu.VMEM)
-    width = rows.shape[1]
+    hbm = pl.BlockSpec(memory_space=pl.ANY)
+    count, width = resid.shape
+    line, plane = seq // 2, 2 * ranks
+    cap = 2 * count * top // (seq * ranks)
+    pieces = 4
+    packed = pltpu.VMEM((line, plane, cap, width), jnp.bfloat16)
+    lined = pltpu.VMEM((line, count, width), jnp.bfloat16)
+    copies = pltpu.SemaphoreType.DMA
+    inner = (max(plane * cap, count), max(experts[0].shape[1], shared[0].shape[1]))
     return pl.pallas_call(
-        functools.partial(dispatch_kernel, seq, ranks),
-        out_shape=jax.ShapeDtypeStruct((ranks, seq, capacity, width), rows.dtype),
-        in_specs=[vmem] * 2,
+        functools.partial(moe_kernel, seq, ranks, top, cap),
+        out_shape=jax.ShapeDtypeStruct(resid.shape, resid.dtype),
+        in_specs=[vmem] * 3 + [hbm] * 6,
         out_specs=vmem,
-        scratch_shapes=[
-            pltpu.VMEM((seq,) + rows.shape, rows.dtype),
-            pltpu.VMEM((seq, ranks, capacity, width), rows.dtype),
-            pltpu.SemaphoreType.DMA((seq,)),
-            pltpu.SemaphoreType.DMA((seq,)),
-            pltpu.SemaphoreType.DMA((seq, ranks)),
-            pltpu.SemaphoreType.DMA((ranks,)),
+        scratch_shapes=[pltpu.VMEM(w.shape, w.dtype) for w in experts + shared]
+        + [lined]
+        + [packed] * 4
+        + [
+            lined,
+            pltpu.VMEM((line + 1, count, width), jnp.bfloat16),
+            pltpu.VMEM((count, width), jnp.float32),
+            pltpu.VMEM(inner, jnp.bfloat16),
+            copies((6,)),
+            copies((line, 2)),
+            copies((line,)),
+            copies((line, plane)),
+            copies((line,)),
+            copies((line, plane)),
+            copies((line,)),
+            copies((line, pieces)),
+            copies((line + 1, pieces)),
         ],
         compiler_params=pltpu.CompilerParams(collective_id=2, has_side_effects=True),
-        name="dispatch",
-    )(rows, pick)
-
-
-def combine_kernel(seq, ranks, done_ref, gate_ref, out_ref, back, lent, landed, finished, arrived,
-                   t_send, t_recv, y_send, y_recv, z_send, z_recv):
-    me, rank = lax.axis_index("sp"), lax.axis_index("tp")
-    partner = me + 1 - 2 * (me % 2)
-    capacity, width = done_ref.shape[2:]
-    steps = seq // 2
-    slots = ranks * capacity
-    greet(seq, ranks, me, rank)
-
-    def hand(block, step):
-        target = (rank + step) % ranks
-        return pltpu.make_async_remote_copy(
-            src_ref=done_ref.at[target, block],
-            dst_ref=back.at[block, rank],
-            send_sem=t_send.at[block, step],
-            recv_sem=t_recv.at[block],
-            device_id={"tp": target},
-            device_id_type=MESH,
-        )
-
-    def lend(block, step):
-        return pltpu.make_async_remote_copy(
-            src_ref=lent.at[step],
-            dst_ref=landed.at[step],
-            send_sem=y_send.at[step],
-            recv_sem=y_recv.at[step],
-            device_id={"sp": partner},
-            device_id_type=MESH,
-        )
-
-    def give(step):
-        return pltpu.make_async_remote_copy(
-            src_ref=finished.at[step],
-            dst_ref=arrived.at[step],
-            send_sem=z_send.at[step],
-            recv_sem=z_recv.at[step],
-            device_id={"sp": (me + 2 * step) % seq},
-            device_id_type=MESH,
-        )
-
-    order = list(range(1, steps)) + [0]
-    for turn in order:
-        for base in (partner, me):
-            block = (base + 2 * turn) % seq
-            for step in range(1, ranks):
-                hand(block, step).start()
-            back[block, rank] = done_ref[rank, block]
-
-    def await_back(block):
-        pltpu.make_async_remote_copy(
-            src_ref=back.at[block, pl.ds(0, ranks - 1)],
-            dst_ref=back.at[block, pl.ds(0, ranks - 1)],
-            send_sem=t_send.at[block, 0],
-            recv_sem=t_recv.at[block],
-            device_id={"sp": partner},
-            device_id_type=MESH,
-        ).wait_recv()
-
-    def weighted(block, columns):
-        rows = jnp.concatenate([back[block, t, :, columns] for t in range(ranks)], axis=0)
-        return jnp.dot(
-            gate_ref[block, :, 0:slots], rows, preferred_element_type=jnp.float32
-        ) + jnp.dot(gate_ref[block, :, slots:], rows, preferred_element_type=jnp.float32)
-
-    for turn in order:
-        block = (partner + 2 * turn) % seq
-        await_back(block)
-        for start in range(0, width, 512):
-            columns = slice(start, start + 512)
-            lent[turn, :, columns] = weighted(block, columns).astype(jnp.bfloat16)
-        lend(block, turn).start()
-        block = (me + 2 * turn) % seq
-        await_back(block)
-        lend(block, turn).wait_recv()
-        for start in range(0, width, 512):
-            columns = slice(start, start + 512)
-            here = weighted(block, columns) + landed[turn, :, columns].astype(jnp.float32)
-            if turn:
-                finished[turn, :, columns] = here.astype(jnp.bfloat16)
-            else:
-                out_ref[:, columns] = here
-        if turn:
-            give(turn).start()
-    for turn in range(1, steps):
-        give(turn).wait_recv()
-        out_ref[...] += arrived[turn].astype(jnp.float32)
-    for turn in range(steps):
-        lend(me, turn).wait_send()
-        if turn:
-            give(turn).wait_send()
-    for block in range(seq):
-        for step in range(1, ranks):
-            hand(block, step).wait_send()
-
-
-def combine(done, gate, seq, ranks):
-    vmem = pl.BlockSpec(memory_space=pltpu.VMEM)
-    capacity, width = done.shape[2:]
-    rows = gate.shape[1]
-    steps = seq // 2
-    return pl.pallas_call(
-        functools.partial(combine_kernel, seq, ranks),
-        out_shape=jax.ShapeDtypeStruct((rows, width), jnp.float32),
-        in_specs=[vmem] * 2,
-        out_specs=vmem,
-        scratch_shapes=[pltpu.VMEM((seq, ranks, capacity, width), done.dtype)]
-        + [pltpu.VMEM((steps, rows, width), done.dtype)] * 4
-        + [
-            pltpu.SemaphoreType.DMA((seq, ranks)),
-            pltpu.SemaphoreType.DMA((seq,)),
-        ]
-        + [pltpu.SemaphoreType.DMA((steps,))] * 4,
-        compiler_params=pltpu.CompilerParams(collective_id=3, has_side_effects=True),
-        name="combine",
-    )(done, gate)
-
-
-def expert_rows(arrived, w_gate, w_up, w_down):
-    gate_part = jnp.einsum("nd,df->nf", arrived, w_gate, preferred_element_type=jnp.float32)
-    up_part = jnp.einsum("nd,df->nf", arrived, w_up, preferred_element_type=jnp.float32)
-    inner = (jax.nn.silu(gate_part) * up_part).astype(jnp.bfloat16)
-    return jnp.einsum("nf,fd->nd", inner, w_down, preferred_element_type=jnp.float32).astype(
-        jnp.bfloat16
-    )
+        name="moe",
+    )(resid, gain, plans, *experts, *shared)
 
 
 def body(
@@ -598,43 +688,20 @@
     slot_ids = (flat_expert * capacity + rank).reshape(row_count, top_count)
     route_plan = jnp.concatenate([slot_ids.astype(jnp.float32).T, gates.T], axis=0)
     every, far, plans = gather_keys(packed, queries, route_plan, seq_count)
-    group_slots = rank_count * capacity
-    near = (
-        plans[:, :top_count].astype(jnp.int32) - lax.axis_index("sp") * group_slots
-    )
-    slot_grid = jnp.arange(group_slots, dtype=jnp.int32)
-    pick = jnp.any(near[:, :, None, :] == slot_grid[None, None, :, None], axis=1).astype(
-        jnp.bfloat16
-    )
-    weight = jnp.sum(
-        jnp.where(
-            near[:, :, :, None] == slot_grid[None, None, None, :],
-            plans[:, top_count:, :, None],
-            0.0,
-        ),
-        axis=1,
-    )
-    coarse = weight.astype(jnp.bfloat16)
-    fine = (weight - coarse.astype(jnp.float32)).astype(jnp.bfloat16)
-    gate_grid = jnp.concatenate([coarse, fine], axis=2)
     attended = stick_attention(queries, far, every, group_size, head_size, bias_rows)
     token_heads = to_owners(attended, seq_count, rank_count)
     mixed = jnp.dot(token_heads, out_proj, preferred_element_type=jnp.float32)
     resid = (stream.astype(jnp.float32) + mixed).astype(jnp.bfloat16)
-    wide = resid.astype(jnp.float32)
-    factor = lax.rsqrt(jnp.mean(wide * wide, axis=-1, keepdims=True) + 1e-06)
-    normed = (wide * factor * ffn_gain).astype(jnp.bfloat16)
-    arrived = dispatch(normed, pick, seq_count, rank_count, capacity)
-    done = expert_rows(
-        arrived.reshape(-1, arrived.shape[-1]), expert_gate[0], expert_up[0], expert_down[0]
+    return moe(
+        resid,
+        ffn_gain[None, :],
+        plans,
+        (expert_gate[0], expert_up[0], expert_down[0]),
+        (shared_gate, shared_up, shared_down),
+        seq_count,
+        rank_count,
+        top_count,
     )
-    routed = combine(done.reshape(arrived.shape), gate_grid, seq_count, rank_count)
-    shared_inner = (
-        jax.nn.silu(jnp.dot(normed, shared_gate, preferred_element_type=jnp.float32))
-        * jnp.dot(normed, shared_up, preferred_element_type=jnp.float32)
-    ).astype(jnp.bfloat16)
-    shared_out = jnp.dot(shared_inner, shared_down, preferred_element_type=jnp.float32)
-    return (wide + shared_out + routed).astype(jnp.bfloat16)
 
 
 def solution(mesh):

time: 172 us -> 125 us (0.73); the launches traced: 169 us -> 124 us
  Pallas kernels: 137 us -> 110 us
  matrix products: 21.9 us -> 5.76 us
  other arithmetic: 7.93 us -> 4.73 us
    pallas_call x2 -> x1, Pallas kernels: 91.7 us -> 64.7 us  [moe(): pl.pallas_call(functools.partial(moe_kernel, seq, ranks, top, cap), out_s...]
    dot_general x4 -> x0, matrix products: 16.7 us -> none  [the longest x1 6.27 us: expert_rows(): jnp.einsum('nf,fd->nd', inner, w_down, preferred_element_type=jnp.float32)]
where the time goes in v1:
time: 125 us; the launch traced here: 124 us
  Pallas kernels  110 us (88%)
  matrix products  5.76 us (5%)
  other arithmetic  4.73 us (4%)
  local copies, waits for them, and re-layouts  3.97 us (3%)
    pallas_call x1, Pallas kernels, moe(): pl.pallas_call(functools.partial(moe_kernel, seq, ranks, top, cap), out_s...  64.7 us
    pallas_call x1, Pallas kernels, gather_keys(): pl.pallas_call(functools.partial(gather_kernel, seq, half), out_shape=(ja...  17.8 us
    pallas_call x1, Pallas kernels, to_owners(): pl.pallas_call(functools.partial(owners_kernel, seq, ranks), out_shape=ja...  16.9 us
    pallas_call x1, Pallas kernels, stick_attention(): pl.pallas_call(functools.partial(stick_kernel, seq, heads, head_size, bia...  10.4 us
    dot_general x1, matrix products, body(): mixed = jnp.dot(token_heads, out_proj, preferred_element_type=jnp.float32)  5.76 us
    unnamed x5, local copies, waits for them, and re-layouts  3.38 us

profile of v1, /device:TPU:25, one launch (start us, length us, event | category | flops | bytes accessed | tf_op | source)
XLA Modules:
  0.0 124.3 jit_solution(3268892988339940947)
XLA Ops:
  0.0 0.7 reduce_sum.22
  0.7 0.7 divide_bitcast_fusion
  1.4 0.7 fusion.9
  2.1 0.8 copy.17
  2.9 0.1 eq.29
  3.0 0.1 eq.25
  3.1 0.6 reduce-window.6
  3.7 0.2 slice_reduce_fusion
  3.9 0.1 fusion.7
  4.0 0.1 reduce_sum.21
  4.1 0.1 copy.20
  4.2 0.7 convert_bitcast_fusion
  4.9 0.6 pad_maximum_fusion.route_ref
  5.5 0.9 copy.16
  6.4 0.6 fusion.4.packed_ref
  7.1 17.8 %gather_keys.1 = (bf16[8,144,256]{2,1,0:T(8,128)(2,1)}, bf16[128,512]{1,0:T(8,128)(2,1)}, f32[8,8,64]{2,1,0:T(8,128)}) custom-call(bf16[144,256]{1,0:T(8,128)(2,1)} %fusion.4.packed_ref, bf16[256,512]{1,0:T(8,128)(2,1)} %query_ref.3, f32[8,64]{1,0:T(8,128)} %pad_maximum_fusion.route_ref), custom_call_target="tpu_custom_call" | custom-call | tf_op jit(solution)/shard_map/gather_keys/pallas_call | solution.py:100
  24.9 0.0 copy-start
  24.9 10.4 %stick_attention.1.part_ref = bf16[256,512]{1,0:T(8,128)(2,1)} custom-call(bf16[256,512]{1,0:T(8,128)(2,1)} %query_ref.3, bf16[128,512]{1,0:T(8,128)(2,1)} %get-tuple-element.8.far_ref, bf16[8,144,256]{2,1,0:T(8,128)(2,1)} %get-tuple-element.9.every_ref), custom_call_target="tpu_custom_call" | custom-call | flops 1811939328 | bytes 589824 | tf_op jit(solution)/shard_map/stick_attention/pallas_call | solution.py:203
  35.3 16.9 %to_owners.1 = bf16[64,2048]{1,0:T(8,128)(2,1)} custom-call(bf16[256,512]{1,0:T(8,128)(2,1)} %stick_attention.1.part_ref), custom_call_target="tpu_custom_call" | custom-call | tf_op jit(solution)/shard_map/to_owners/pallas_call | solution.py:305
  52.2 0.0 copy-done
  52.2 5.8 %fusion.resid_ref = bf16[64,2048]{1,0:T(8,128)(2,1)} fusion(bf16[64,2048]{1,0:T(8,128)(2,1)} %to_owners.1, bf16[2048,2048]{1,0:T(8,128)(2,1)} %param.18, bf16[64,2048]{1,0:T(8,128)(2,1)S(1)} %copy-done), kind=kOutput, calls=%fused_computation.1 | convolution fusion | flops 537264128 | bytes 9175040 | tf_op jit(solution)/shard_map/dot_general | solution.py:693
  58.0 64.7 %moe.1 = bf16[64,2048]{1,0:T(8,128)(2,1)} custom-call(bf16[64,2048]{1,0:T(8,128)(2,1)} %fusion.resid_ref, f32[1,2048]{1,0:T(1,128)} %bitcast.38, f32[8,8,64]{2,1,0:T(8,128)} %get-tuple-element.10.plans_ref, bf16[2048,512]{1,0:T(8,128)(2,1)} %bitcast.34, bf16[2048,512]{1,0:T(8,128)(2,1)} %bitcast.35, bf16[512,2048]{1,0:T(8,128)(2,1)} %bitcast.36, ...), custom_call_target="tpu_custom_call" | custom-call | tf_op jit(solution)/shard_map/moe/pallas_call | solution.py:619
  122.7 1.7 %copy.24 = bf16[64,2048]{1,0:T(8,128)(2,1)} copy(bf16[64,2048]{1,0:T(8,128)(2,1)} %moe.1) | data formatting | bytes 524288
  (4 shorter events, 0.1 us)
Async XLA Ops:
  24.9 27.3 %copy-start = (bf16[64,2048]{1,0:T(8,128)(2,1)S(1)}, bf16[64,2048]{1,0:T(8,128)(2,1)}, u32[]{:S(2)}) copy-start(bf16[64,2048]{1,0:T(8,128)(2,1)} %param.17) | copy-start | bytes 786436
